TPU v7x, 32 devices: a whole 2x2x4 slice. The times are simulated.
32 devices in a mesh: rep: 8 (over z, y), fs: 2 (over x), tp: 2 (over core).
Axes of the slice: x: 2, y: 2, z: 4, core: 2. Of those that a mesh axis runs over, the one named last changes fastest.
Arguments:
- inputs: bfloat16 [4096, 2048], P(('rep', 'tp'), 'fs'), may hold values from -6 to 6
- pre_act: bfloat16 [4096, 4096], P(('rep', 'fs'), 'tp'), may hold values from -6 to 6
- cotangent: bfloat16 [4096, 2048], P(('rep', 'tp'), 'fs'), may hold values from -6 to 6
- up_weight: bfloat16 [2048, 4096], P('fs', 'tp'), may hold values from -0.125 to 0.125
- down_weight: bfloat16 [4096, 2048], P('tp', 'fs'), may hold values from -0.09375 to 0.09375
Outputs:
- grad_inputs: bfloat16 [4096, 2048], P(('rep', 'tp'), 'fs')
- grad_up: float32 [2048, 4096], P('fs', 'tp')
- grad_down: float32 [4096, 2048], P('tp', 'fs')
All inputs are finite; a program needn't handle non-finite values.
Results may differ from a plain program's by a relative error of at most 0.015.
Values may be sent and summed in bfloat16 or wider, within the bound.
A program may use at most 128 MiB of HBM per device.

v0:
```python
import jax
import jax.numpy as jnp
from jax import lax
from jax.sharding import PartitionSpec as P


def contract_rows(left, right):
    return lax.dot_general(
        left, right, (((0,), (0,)), ((), ())), preferred_element_type=jnp.float32
    )


def contract_cols(left, right):
    return lax.dot_general(
        left, right, (((1,), (1,)), ((), ())), preferred_element_type=jnp.float32
    )


def per_device(inputs, pre_act, cotangent, up_weight, down_weight):
    group_x, group_cot = (
        lax.all_gather(inputs, "tp", axis=0, tiled=True),
        lax.all_gather(cotangent, "tp", axis=0, tiled=True),
    )
    positive = jnp.maximum(pre_act.astype(jnp.float32), 0.0)
    square = (positive * positive).astype(jnp.bfloat16)
    rows_block = group_cot
    grad_act = lax.psum_scatter(
        contract_cols(rows_block, down_weight).astype(jnp.bfloat16),
        "fs",
        scatter_dimension=0,
        tiled=True,
    ).astype(jnp.float32)
    grad_pre = (2.0 * positive * grad_act).astype(jnp.bfloat16)
    factor = (inputs.shape[0] * lax.axis_size("rep") * lax.axis_size("tp")) ** (-0.5)
    group_grad, group_square = (
        lax.all_gather(grad_pre, "fs", axis=0, tiled=True),
        lax.all_gather(square, "fs", axis=0, tiled=True),
    )
    down_part = contract_rows(group_square, group_cot)
    up_part = contract_rows(group_x, group_grad)
    up_slice, down_slice = (
        lax.psum_scatter(up_part, "rep", scatter_dimension=0, tiled=True),
        lax.psum_scatter(down_part, "rep", scatter_dimension=0, tiled=True),
    )
    grad_up, grad_down = (
        lax.all_gather(up_slice.astype(jnp.bfloat16), "rep", axis=0, tiled=True).astype(
            up_slice.dtype
        ),
        lax.all_gather(down_slice.astype(jnp.bfloat16), "rep", axis=0, tiled=True).astype(
            down_slice.dtype
        ),
    )
    rows_block = group_grad
    grad_inputs = lax.psum_scatter(
        contract_cols(rows_block, up_weight).astype(jnp.bfloat16),
        "tp",
        scatter_dimension=0,
        tiled=True,
    )
    return (grad_inputs, grad_up * factor, grad_down * factor)


def solution(mesh):
    placed = (
        P(("rep", "tp"), "fs"),
        P(("rep", "fs"), "tp"),
        P(("rep", "tp"), "fs"),
        P("fs", "tp"),
        P("tp", "fs"),
    )
    return jax.shard_map(
        per_device,
        mesh=mesh,
        in_specs=placed,
        out_specs=(P(("rep", "tp"), "fs"), P("fs", "tp"), P("tp", "fs")),
        check_vma=False,
    )
```

profile of v0, /device:TPU:0, one launch (start us, length us, event | category | flops | bytes accessed | tf_op | source)
XLA Modules:
  0.0 611.5 jit_solution(11408372984345961125)
XLA Ops:
  7.2 0.7 all-gather.7.cloned.1.call-update
  7.9 0.0 reduce-scatter.5.cloned.1.call-start
  8.0 13.3 %all-gather.7.cloned.1.call-done = bf16[512,1024]{1,0:T(8,128)(2,1)} async-done(((bf16[256,1024]{1,0:T(8,128)(2,1)}), bf16[512,1024]{1,0:T(8,128)(2,1)}) %all-gather.7.cloned.1.call-update) | async-done | bytes 1048592 | tf_op jit(solution)/shard_map/all_gather | solution.py:22
  21.3 6.2 %convolution_convert_fusion = bf16[512,2048]{1,0:T(8,128)(2,1)} fusion(bf16[512,1024]{1,0:T(8,128)(2,1)} %all-gather.7.cloned.1.call-done, bf16[2048,1024]{1,0:T(8,128)(2,1)} %param.9), kind=kOutput, calls=%fused_computation.3 | convolution fusion | flops 2148532224 | bytes 7340032 | tf_op jit(solution)/shard_map/dot_general | solution.py:14
  27.5 0.0 all-gather.11.cloned.1.call-start
  27.6 0.7 all-gather.11.cloned.1.call-update
  28.3 0.0 all-gather.9.cloned.1.call-start
  28.3 32.5 %reduce-scatter.5.cloned.1.call-done = bf16[256,2048]{1,0:T(8,128)(2,1)} async-done(((bf16[512,2048]{1,0:T(8,128)(2,1)}), bf16[256,2048]{1,0:T(8,128)(2,1)}) %reduce-scatter.5.cloned.1.call-update) | async-done | bytes 1048592 | tf_op jit(solution)/shard_map/reduce_scatter | solution.py:27
  60.8 3.1 multiply_convert_fusion
  63.9 0.0 all-gather.15.cloned.1.call-start
  64.0 0.5 all-gather.15.cloned.1.call-update
  64.5 0.0 reduce-scatter.9.cloned.1.call-start
  64.5 6.8 %all-gather.11.cloned.1.call-done = bf16[512,1024]{1,0:T(8,128)(2,1)} async-done(((bf16[256,1024]{1,0:T(8,128)(2,1)}), bf16[512,1024]{1,0:T(8,128)(2,1)}) %all-gather.11.cloned.1.call-update) | async-done | bytes 1048592 | tf_op jit(solution)/shard_map/all_gather | solution.py:21
  71.4 36.3 %all-gather.9.cloned.1.call-done = bf16[512,2048]{1,0:T(8,128)(2,1)} async-done(((bf16[256,2048]{1,0:T(8,128)(2,1)}), bf16[512,2048]{1,0:T(8,128)(2,1)}) %all-gather.9.cloned.1.call-update) | async-done | bytes 2097168 | tf_op jit(solution)/shard_map/all_gather | solution.py:36
  107.7 7.6 %convolution_bitcast_fusion = f32[1024,2048]{0,1:T(8,128)} fusion(bf16[512,2048]{1,0:T(8,128)(2,1)} %all-gather.9.cloned.1.call-done, bf16[512,1024]{1,0:T(8,128)(2,1)} %all-gather.11.cloned.1.call-done), kind=kOutput, calls=%fused_computation.2 | convolution fusion | flops 2147483648 | bytes 11534336 | tf_op jit(solution)/shard_map/dot_general | solution.py:8
  115.3 0.0 reduce-scatter.11.cloned.1.call-start
  115.4 27.4 %all-gather.15.cloned.1.call-done = bf16[512,2048]{1,0:T(8,128)(2,1)} async-done(((bf16[256,2048]{1,0:T(8,128)(2,1)}), bf16[512,2048]{1,0:T(8,128)(2,1)}) %all-gather.15.cloned.1.call-update) | async-done | bytes 2097168 | tf_op jit(solution)/shard_map/all_gather | solution.py:37
  142.7 7.4 %fusion = f32[2048,1024]{1,0:T(8,128)} fusion(bf16[512,2048]{1,0:T(8,128)(2,1)} %all-gather.15.cloned.1.call-done, bf16[512,1024]{1,0:T(8,128)(2,1)S(1)} %copy-done.2), kind=kOutput, calls=%fused_computation.8 | convolution fusion | flops 2147483648 | bytes 11534336 | tf_op jit(solution)/shard_map/dot_general | solution.py:8
  150.1 0.0 all-gather.13.cloned.1.call-start
  150.2 144.5 %reduce-scatter.9.cloned.1.call-done = f32[128,2048]{0,1:T(8,128)} async-done(((f32[1024,2048]{0,1:T(8,128)}), f32[128,2048]{0,1:T(8,128)}) %reduce-scatter.9.cloned.1.call-update) | async-done | bytes 1048592 | tf_op jit(solution)/shard_map/reduce_scatter | solution.py:42
  294.7 2.1 convert_element_type.35
  296.8 0.0 all-gather.17.cloned.1.call-start
  296.8 148.7 %reduce-scatter.11.cloned.1.call-done = f32[256,1024]{1,0:T(8,128)} async-done(((f32[2048,1024]{1,0:T(8,128)}), f32[256,1024]{1,0:T(8,128)}) %reduce-scatter.11.cloned.1.call-update) | async-done | bytes 1048592 | tf_op jit(solution)/shard_map/reduce_scatter | solution.py:43
  445.5 2.1 convert_element_type.38
  447.6 0.2 reduce-scatter.7.cloned.1.call-start
  447.9 5.6 convolution_convert_fusion.1
  453.5 68.4 %all-gather.13.cloned.1.call-done = bf16[1024,2048]{0,1:T(8,128)(2,1)} async-done(((bf16[128,2048]{0,1:T(8,128)(2,1)}), bf16[1024,2048]{0,1:T(8,128)(2,1)}) %all-gather.13.cloned.1.call-update) | async-done | bytes 4194320 | tf_op jit(solution)/shard_map/all_gather | solution.py:46
  521.9 6.8 %convert_multiply_fusion.1 = f32[1024,2048]{0,1:T(8,128)} fusion(bf16[1024,2048]{0,1:T(8,128)(2,1)} %all-gather.13.cloned.1.call-done), kind=kLoop, calls=%fused_computation.1 | loop fusion | flops 4194304 | bytes 12582912 | tf_op jit(solution)/shard_map/mul | solution.py:60
  528.7 9.3 %copy.8 = f32[1024,2048]{1,0:T(8,128)} copy(f32[1024,2048]{0,1:T(8,128)} %convert_multiply_fusion.1) | data formatting | bytes 16777216
  538.0 57.1 %all-gather.17.cloned.1.call-done = bf16[2048,1024]{1,0:T(8,128)(2,1)} async-done(((bf16[256,1024]{1,0:T(8,128)(2,1)}), bf16[2048,1024]{1,0:T(8,128)(2,1)}) %all-gather.17.cloned.1.call-update) | async-done | bytes 4194320 | tf_op jit(solution)/shard_map/all_gather | solution.py:49
  595.0 6.8 %convert_multiply_fusion = f32[2048,1024]{1,0:T(8,128)} fusion(bf16[2048,1024]{1,0:T(8,128)(2,1)} %all-gather.17.cloned.1.call-done), kind=kLoop, calls=%fused_computation | loop fusion | flops 4194304 | bytes 12582912 | tf_op jit(solution)/shard_map/mul | solution.py:60
  601.8 2.8 reduce-scatter.7.cloned.1.call-done
  (14 shorter events, 0.2 us)
Async XLA Ops:
  7.2 14.1 %all-gather.7.cloned.1.call-start = ((), (), s32[]{:S(2)}) async-start(), calls=%async_computation.4 | async-start | bytes 1572864 | tf_op jit(solution)/shard_map/all_gather | solution.py:22
  7.9 52.9 %copy-start = (bf16[256,2048]{1,0:T(8,128)(2,1)S(1)}, bf16[256,2048]{1,0:T(8,128)(2,1)}, u32[]{:S(2)}) copy-start(bf16[256,2048]{1,0:T(8,128)(2,1)} %param.6) | copy-start | bytes 3145732
  7.9 52.9 %reduce-scatter.5.cloned.1.call-start = ((), (), s32[]{:S(2)}) async-start(), calls=%async_computation.5 | async-start | bytes 3145728 | tf_op jit(solution)/shard_map/reduce_scatter | solution.py:27
  27.5 43.9 %all-gather.11.cloned.1.call-start = ((), (), s32[]{:S(2)}) async-start(), calls=%async_computation.8 | async-start | bytes 1572864 | tf_op jit(solution)/shard_map/all_gather | solution.py:21
  28.3 79.4 %all-gather.9.cloned.1.call-start = ((), (), s32[]{:S(2)}) async-start(), calls=%async_computation.6 | async-start | bytes 3145728 | tf_op jit(solution)/shard_map/all_gather | solution.py:36
  63.9 78.8 %all-gather.15.cloned.1.call-start = ((), (), s32[]{:S(2)}) async-start(), calls=%async_computation.11 | async-start | bytes 3145728 | tf_op jit(solution)/shard_map/all_gather | solution.py:37
  64.5 230.2 %reduce-scatter.9.cloned.1.call-start = ((), (), s32[]{:S(2)}) async-start(), calls=%async_computation.9 | async-start | bytes 9437184 | tf_op jit(solution)/shard_map/reduce_scatter | solution.py:42
  115.3 27.5 %copy-start.2 = (bf16[512,1024]{1,0:T(8,128)(2,1)S(1)}, bf16[512,1024]{1,0:T(8,128)(2,1)}, u32[]{:S(2)}) copy-start(bf16[512,1024]{1,0:T(8,128)(2,1)} %all-gather.7.cloned.1.call-done) | copy-start | bytes 3145732
  115.3 330.2 %reduce-scatter.11.cloned.1.call-start = ((), (), s32[]{:S(2)}) async-start(), calls=%async_computation.12 | async-start | bytes 9437184 | tf_op jit(solution)/shard_map/reduce_scatter | solution.py:43
  150.1 297.7 %copy-start.1 = (bf16[512,2048]{1,0:T(8,128)(2,1)S(1)}, bf16[512,2048]{1,0:T(8,128)(2,1)}, u32[]{:S(2)}) copy-start(bf16[512,2048]{1,0:T(8,128)(2,1)} %all-gather.9.cloned.1.call-done) | copy-start | bytes 6291460
  150.1 371.7 %all-gather.13.cloned.1.call-start = ((), (), s32[]{:S(2)}) async-start(), calls=%async_computation.10 | async-start | bytes 4718592 | tf_op jit(solution)/shard_map/all_gather | solution.py:46
  296.8 298.2 %all-gather.17.cloned.1.call-start = ((), (), s32[]{:S(2)}) async-start(), calls=%async_computation.13 | async-start | bytes 4718592 | tf_op jit(solution)/shard_map/all_gather | solution.py:49
  447.6 157.0 %reduce-scatter.7.cloned.1.call-start = ((), (), s32[]{:S(2)}) async-start(), calls=%async_computation.7 | async-start | bytes 1572864 | tf_op jit(solution)/shard_map/reduce_scatter | solution.py:54
Sparse Core Ops, SparseCore 0:
  9.5 11.7 all-gather.6
  27.6 33.0 reduce-scatter.4
  62.3 9.0 all-gather.10
  73.4 34.2 all-gather.8
  109.6 33.0 all-gather.14
  146.8 147.8 reduce-scatter.8
  298.9 146.5 reduce-scatter.10
  448.1 73.7 all-gather.12
  524.0 70.9 all-gather.16
  597.7 6.8 reduce-scatter.6
where the time goes:
time: 612 us; the launch traced here: 611 us
  waiting for transfers between devices  540 us (88%)
  matrix products  26.8 us (4%)
  other arithmetic  20.9 us (3%)
  between operations  14.2 us (2%)
  local copies, waits for them, and re-layouts  9.29 us (2%)
    reduce_scatter x1, waiting for transfers between devices, per_device(): lax.psum_scatter(down_part, 'rep', scatter_dimension=0, tiled=True)  149 us
    reduce_scatter x1, waiting for transfers between devices, per_device(): lax.psum_scatter(up_part, 'rep', scatter_dimension=0, tiled=True)  144 us
    all_gather x1, waiting for transfers between devices, per_device(): lax.all_gather(up_slice.astype(jnp.bfloat16), 'rep', axis=0, tiled=True)  68.4 us
    all_gather x1, waiting for transfers between devices, per_device(): lax.all_gather(down_slice.astype(jnp.bfloat16), 'rep', axis=0, tiled=True)  57.1 us
    all_gather x1, waiting for transfers between devices, per_device(): lax.all_gather(grad_pre, 'fs', axis=0, tiled=True)  36.3 us
    reduce_scatter x1, waiting for transfers between devices, per_device(): lax.psum_scatter(contract_cols(rows_block, down_weight).astype(jnp.bfloat...  32.5 us
    all_gather x1, waiting for transfers between devices, per_device(): lax.all_gather(square, 'fs', axis=0, tiled=True)  27.4 us
    dot_general x2, matrix products, contract_rows(): lax.dot_general(left, right, (((0,), (0,)), ((), ())), preferred_element_...  15 us
  transfers between devices with their start and end apart: 10, of which 10 were waited for; matrix products, arithmetic and copies ran while one was open for 8% of the time, Pallas kernels for 0%

commit v1 on v0

--- a/solution.py
+++ b/solution.py
@@ -33,7 +33,9 @@
     grad_pre = (2.0 * positive * grad_act).astype(jnp.bfloat16)
     factor = (inputs.shape[0] * lax.axis_size("rep") * lax.axis_size("tp")) ** (-0.5)
     group_grad, group_square = (
-        lax.all_gather(grad_pre, "fs", axis=0, tiled=True),
+        jnp.concatenate(
+            lax.all_to_all(jnp.stack([grad_pre] * lax.axis_size("fs")), "fs", 0, 0), axis=0
+        ),
         lax.all_gather(square, "fs", axis=0, tiled=True),
     )
     down_part = contract_rows(group_square, group_cot)

time: 612 us -> 585 us (0.956)
  waiting for transfers between devices: 540 us -> 509 us
    all_gather x1 -> x0, waiting for transfers between devices: 36.3 us -> none  [per_device(): lax.all_gather(grad_pre, 'fs', axis=0, tiled=True)]
    all_to_all x0 -> x1, waiting for transfers between devices: none -> 32.5 us  [per_device(): lax.all_to_all(jnp.stack([grad_pre] * lax.axis_size('fs')), 'fs', 0, 0)]
    all_gather x1, waiting for transfers between devices: 27.4 us -> 5.54 us  [per_device(): lax.all_gather(square, 'fs', axis=0, tiled=True)]
  transfers between devices with their start and end apart: 10 -> 10, of which waited for: 10 -> 10; matrix products, arithmetic and copies ran while one was open for 8% -> 9% of each run, Pallas kernels for 0% -> 0%
where the time goes in v1:
time: 585 us
  waiting for transfers between devices  509 us (87%)
  matrix products  26.2 us (4%)
  other arithmetic  22 us (4%)
  between operations  13.9 us (2%)
  local copies, waits for them, and re-layouts  9.29 us (2%)
    reduce_scatter x1, waiting for transfers between devices, per_device(): lax.psum_scatter(down_part, 'rep', scatter_dimension=0, tiled=True)  149 us
    reduce_scatter x1, waiting for transfers between devices, per_device(): lax.psum_scatter(up_part, 'rep', scatter_dimension=0, tiled=True)  144 us
    all_gather x1, waiting for transfers between devices, per_device(): lax.all_gather(up_slice.astype(jnp.bfloat16), 'rep', axis=0, tiled=True)  68.4 us
    all_gather x1, waiting for transfers between devices, per_device(): lax.all_gather(down_slice.astype(jnp.bfloat16), 'rep', axis=0, tiled=True)  57.1 us
    all_to_all x1, waiting for transfers between devices, per_device(): lax.all_to_all(jnp.stack([grad_pre] * lax.axis_size('fs')), 'fs', 0, 0)  32.5 us
    reduce_scatter x1, waiting for transfers between devices, per_device(): lax.psum_scatter(contract_cols(rows_block, down_weight).astype(jnp.bfloat...  32.5 us
    dot_general x2, matrix products, contract_rows(): lax.dot_general(left, right, (((0,), (0,)), ((), ())), preferred_element_...  14.4 us
    mul x2, other arithmetic, per_device(): return (grad_inputs, grad_up * factor, grad_down * factor)  13.6 us
  transfers between devices with their start and end apart: 10, of which 10 were waited for; matrix products, arithmetic and copies ran while one was open for 9% of the time, Pallas kernels for 0%

profile of v1, /device:TPU:0, one launch (start us, length us, event | category | flops | bytes accessed | tf_op | source)
XLA Modules:
  0.0 584.9 jit_solution(8338524820825390034)
XLA Ops:
  7.2 0.7 all-gather.6.cloned.1.call-update
  7.9 0.0 reduce-scatter.5.cloned.1.call-start
  8.0 13.3 %all-gather.6.cloned.1.call-done = bf16[512,1024]{1,0:T(8,128)(2,1)} async-done(((bf16[256,1024]{1,0:T(8,128)(2,1)}), bf16[512,1024]{1,0:T(8,128)(2,1)}) %all-gather.6.cloned.1.call-update) | async-done | bytes 1048592 | tf_op jit(solution)/shard_map/all_gather | solution.py:22
  21.3 6.2 %convolution_convert_fusion = bf16[512,2048]{1,0:T(8,128)(2,1)} fusion(bf16[512,1024]{1,0:T(8,128)(2,1)} %all-gather.6.cloned.1.call-done, bf16[2048,1024]{1,0:T(8,128)(2,1)} %param.9), kind=kOutput, calls=%fused_computation.3 | convolution fusion | flops 2148532224 | bytes 7340032 | tf_op jit(solution)/shard_map/dot_general | solution.py:14
  27.5 0.0 all-gather.8.cloned.1.call-start
  27.6 0.7 all-gather.8.cloned.1.call-update
  28.3 0.0 all-gather.12.cloned.1.call-start
  28.3 32.5 %reduce-scatter.5.cloned.1.call-done = bf16[256,2048]{1,0:T(8,128)(2,1)} async-done(((bf16[512,2048]{1,0:T(8,128)(2,1)}), bf16[256,2048]{1,0:T(8,128)(2,1)}) %reduce-scatter.5.cloned.1.call-update) | async-done | bytes 1048592 | tf_op jit(solution)/shard_map/reduce_scatter | solution.py:27
  60.8 2.8 multiply_convert_fusion
  63.6 1.5 pad_maximum_fusion
  65.1 3.8 all-to-all-start
  68.9 0.0 reduce-scatter.9.cloned.1.call-start
  68.9 2.5 all-gather.8.cloned.1.call-done
  71.4 32.5 %all-to-all-done = bf16[2,256,2048]{2,1,0:T(8,128)(2,1)S(1)} async-done(((bf16[2,256,2048]{2,1,0:T(8,128)(2,1)}), bf16[2,256,2048]{2,1,0:T(8,128)(2,1)S(1)}, u32[]{:S(2)}, u32[]{:S(2)}) %all-to-all-start) | async-done | bytes 2097184 | tf_op jit(solution)/shard_map/all_to_all | solution.py:37
  103.8 7.0 %convolution_bitcast_fusion = f32[1024,2048]{0,1:T(8,128)} fusion(bf16[512,2048]{1,0:T(8,128)(2,1)S(1)} %bitcast.13, bf16[512,1024]{1,0:T(8,128)(2,1)} %all-gather.8.cloned.1.call-done), kind=kOutput, calls=%fused_computation.2 | convolution fusion | flops 2147483648 | bytes 11534336 | tf_op jit(solution)/shard_map/dot_general | solution.py:8
  110.9 0.0 reduce-scatter.11.cloned.1.call-start
  110.9 5.5 all-gather.12.cloned.1.call-done
  116.5 7.4 %fusion.1 = f32[2048,1024]{1,0:T(8,128)} fusion(bf16[512,2048]{1,0:T(8,128)(2,1)} %all-gather.12.cloned.1.call-done, bf16[512,1024]{1,0:T(8,128)(2,1)S(1)} %copy-done.1), kind=kOutput, calls=%fused_computation.10 | convolution fusion | flops 2147483648 | bytes 11534336 | tf_op jit(solution)/shard_map/dot_general | solution.py:8
  123.9 0.0 all-gather.10.cloned.1.call-start
  123.9 144.5 %reduce-scatter.9.cloned.1.call-done = f32[128,2048]{0,1:T(8,128)} async-done(((f32[1024,2048]{0,1:T(8,128)}), f32[128,2048]{0,1:T(8,128)}) %reduce-scatter.9.cloned.1.call-update) | async-done | bytes 1048592 | tf_op jit(solution)/shard_map/reduce_scatter | solution.py:44
  268.4 2.1 convert_element_type.35
  270.5 0.0 all-gather.14.cloned.1.call-start
  270.5 148.5 %reduce-scatter.11.cloned.1.call-done = f32[256,1024]{1,0:T(8,128)} async-done(((f32[2048,1024]{1,0:T(8,128)}), f32[256,1024]{1,0:T(8,128)}) %reduce-scatter.11.cloned.1.call-update) | async-done | bytes 1048592 | tf_op jit(solution)/shard_map/reduce_scatter | solution.py:45
  419.0 2.1 convert_element_type.38
  421.2 0.2 reduce-scatter.7.cloned.1.call-start
  421.4 5.6 convolution_convert_fusion.1
  427.1 68.4 %all-gather.10.cloned.1.call-done = bf16[1024,2048]{0,1:T(8,128)(2,1)} async-done(((bf16[128,2048]{0,1:T(8,128)(2,1)}), bf16[1024,2048]{0,1:T(8,128)(2,1)}) %all-gather.10.cloned.1.call-update) | async-done | bytes 4194320 | tf_op jit(solution)/shard_map/all_gather | solution.py:48
  495.5 6.8 %convert_multiply_fusion.1 = f32[1024,2048]{0,1:T(8,128)} fusion(bf16[1024,2048]{0,1:T(8,128)(2,1)} %all-gather.10.cloned.1.call-done), kind=kLoop, calls=%fused_computation.1 | loop fusion | flops 4194304 | bytes 12582912 | tf_op jit(solution)/shard_map/mul | solution.py:62
  502.2 9.3 %copy.8 = f32[1024,2048]{1,0:T(8,128)} copy(f32[1024,2048]{0,1:T(8,128)} %convert_multiply_fusion.1) | data formatting | bytes 16777216
  511.5 57.1 %all-gather.14.cloned.1.call-done = bf16[2048,1024]{1,0:T(8,128)(2,1)} async-done(((bf16[256,1024]{1,0:T(8,128)(2,1)}), bf16[2048,1024]{1,0:T(8,128)(2,1)}) %all-gather.14.cloned.1.call-update) | async-done | bytes 4194320 | tf_op jit(solution)/shard_map/all_gather | solution.py:51
  568.6 6.8 %convert_multiply_fusion = f32[2048,1024]{1,0:T(8,128)} fusion(bf16[2048,1024]{1,0:T(8,128)(2,1)} %all-gather.14.cloned.1.call-done), kind=kLoop, calls=%fused_computation | loop fusion | flops 4194304 | bytes 12582912 | tf_op jit(solution)/shard_map/mul | solution.py:62
  575.4 3.0 reduce-scatter.7.cloned.1.call-done
  (12 shorter events, 0.2 us)
Async XLA Ops:
  7.2 14.1 %all-gather.6.cloned.1.call-start = ((), (), s32[]{:S(2)}) async-start(), calls=%async_computation.5 | async-start | bytes 1572864 | tf_op jit(solution)/shard_map/all_gather | solution.py:22
  7.9 52.9 %copy-start = (bf16[256,2048]{1,0:T(8,128)(2,1)S(1)}, bf16[256,2048]{1,0:T(8,128)(2,1)}, u32[]{:S(2)}) copy-start(bf16[256,2048]{1,0:T(8,128)(2,1)} %param.6) | copy-start | bytes 3145732
  7.9 52.9 %reduce-scatter.5.cloned.1.call-start = ((), (), s32[]{:S(2)}) async-start(), calls=%async_computation.6 | async-start | bytes 3145728 | tf_op jit(solution)/shard_map/reduce_scatter | solution.py:27
  27.5 43.9 %all-gather.8.cloned.1.call-start = ((), (), s32[]{:S(2)}) async-start(), calls=%async_computation.8 | async-start | bytes 1572864 | tf_op jit(solution)/shard_map/all_gather | solution.py:21
  28.3 88.2 %all-gather.12.cloned.1.call-start = ((), (), s32[]{:S(2)}) async-start(), calls=%async_computation.11 | async-start | bytes 3145728 | tf_op jit(solution)/shard_map/all_gather | solution.py:39
  65.1 38.8 %all-to-all-start = ((bf16[2,256,2048]{2,1,0:T(8,128)(2,1)}), bf16[2,256,2048]{2,1,0:T(8,128)(2,1)S(1)}, u32[]{:S(2)}, u32[]{:S(2)}) async-start(bf16[2,256,2048]{2,1,0:T(8,128)(2,1)} %pad_maximum_fusion), calls=%async_computation.1 | async-start | bytes 4194304 | tf_op jit(solution)/shard_map/all_to_all | solution.py:37
  68.9 199.5 %reduce-scatter.9.cloned.1.call-start = ((), (), s32[]{:S(2)}) async-start(), calls=%async_computation.9 | async-start | bytes 9437184 | tf_op jit(solution)/shard_map/reduce_scatter | solution.py:44
  110.9 5.6 copy-start.1
  110.9 308.2 %reduce-scatter.11.cloned.1.call-start = ((), (), s32[]{:S(2)}) async-start(), calls=%async_computation.12 | async-start | bytes 9437184 | tf_op jit(solution)/shard_map/reduce_scatter | solution.py:45
  123.9 371.6 %all-gather.10.cloned.1.call-start = ((), (), s32[]{:S(2)}) async-start(), calls=%async_computation.10 | async-start | bytes 4718592 | tf_op jit(solution)/shard_map/all_gather | solution.py:48
  270.5 298.1 %all-gather.14.cloned.1.call-start = ((), (), s32[]{:S(2)}) async-start(), calls=%async_computation.13 | async-start | bytes 4718592 | tf_op jit(solution)/shard_map/all_gather | solution.py:51
  421.2 157.2 %reduce-scatter.7.cloned.1.call-start = ((), (), s32[]{:S(2)}) async-start(), calls=%async_computation.7 | async-start | bytes 1572864 | tf_op jit(solution)/shard_map/reduce_scatter | solution.py:56
Sparse Core Ops, SparseCore 0:
  9.5 11.7 all-gather.5
  27.6 33.0 reduce-scatter.4
  62.3 9.0 all-gather.7
  73.4 43.0 all-gather.11
  120.5 147.8 reduce-scatter.8
  272.4 146.5 reduce-scatter.10
  421.7 73.7 all-gather.9
  497.6 70.9 all-gather.13
  571.4 6.8 reduce-scatter.6
